TPU v7x, 32 devices: a whole 2x2x4 slice. The times are simulated.
32 devices in a mesh: ep: 8 (over z, y), tp: 4 (over x, core).
Axes of the slice: x: 2, y: 2, z: 4, core: 2. Of those that a mesh axis runs over, the one named last changes fastest.
Arguments:
- hidden: bfloat16 [256, 2048], P('ep')
- norm_gains: float32 [4, 2048], replicated, may hold values from 0.1 to 1.9
- w_query: bfloat16 [2048, 1024], P(None, 'tp'), may hold values from -0.125 to 0.125
- w_key: bfloat16 [2048, 1024], P(None, 'tp'), may hold values from -0.125 to 0.125
- w_value: bfloat16 [2048, 1024], P(None, 'tp'), may hold values from -0.125 to 0.125
- w_outgate: bfloat16 [2048, 1024], P(None, 'tp'), may hold values from -0.125 to 0.125
- w_input_gate: bfloat16 [2048, 8], replicated, may hold values from -0.125 to 0.125
- w_forget_gate: bfloat16 [2048, 8], replicated, may hold values from -0.125 to 0.125
- forget_bias: float32 [8], replicated, may hold values from -1 to 4
- w_mix_out: bfloat16 [1024, 2048], P('tp')
- state_matrix: float32 [256, 8, 128, 128], P('ep', 'tp'), may hold values from -0.6 to 0.6
- state_norm: float32 [256, 8, 128], P('ep', 'tp'), may hold values from -0.6 to 0.6
- state_max: float32 [256, 8], P('ep', 'tp'), may hold values from -4 to 4
- routes: int32 [256, 2], P('ep'), may hold values from 0 to 7, all different within a row; in each aligned block of 32 rows (0 to 31, 32 to 63, ...) at most 16 rows name the same one
- route_scores: float32 [256, 2], P('ep'), may hold values from 0.1 to 1
- expert_gate: bfloat16 [8, 2048, 3584], P('ep', None, 'tp'), may hold values from -0.125 to 0.125
- expert_up: bfloat16 [8, 2048, 3584], P('ep', None, 'tp'), may hold values from -0.125 to 0.125
- expert_down: bfloat16 [8, 3584, 2048], P('ep', 'tp')
- dense_gate: bfloat16 [2048, 5632], P('tp', 'ep'), may hold values from -0.125 to 0.125
- dense_up: bfloat16 [2048, 5632], P('tp', 'ep'), may hold values from -0.125 to 0.125
- dense_down: bfloat16 [5632, 2048], P('ep', 'tp')
- dense_mix: float32 [2048], replicated, may hold values from -0.25 to 0.25
Outputs:
- new_hidden: bfloat16 [256, 2048], P('ep', 'tp')
- new_matrix: float32 [256, 8, 128, 128], P('ep', 'tp')
- new_norm: float32 [256, 8, 128], P('ep', 'tp')
- new_max: float32 [256, 8], P('ep', 'tp')
Inputs may be any that keep to these rules, and one draw needn't show every extreme that they name: `routes`: each row names 2 different experts. Among the rows of one index of ep (an aligned block of 32 rows) no expert is named by more than 16 rows, and in every draw some expert is named by exactly 16 rows of some block.
All inputs are finite; a program needn't handle non-finite values.
Results may differ from a plain program's by a relative error of at most 0.02.
Values may be sent and summed in bfloat16 or wider, within the bound.
No kernel may reach another device: no remote copies, remote signals or barrier semaphores. Data moves between devices by JAX's collectives and lax.ppermute only.
A program may use at most 128 MiB of HBM per device.

v0:
```python
import jax
import jax.numpy as jnp
from jax import lax
from jax.sharding import PartitionSpec as P

EPS = 1e-06


def settle(values):
    return lax.optimization_barrier(values.astype(jnp.bfloat16)).astype(jnp.float32)


def local(
    hidden,
    norm_gains,
    w_query,
    w_key,
    w_value,
    w_outgate,
    w_input_gate,
    w_forget_gate,
    forget_bias,
    w_mix_out,
    state_matrix,
    state_norm,
    state_max,
    routes,
    route_scores,
    expert_gate,
    expert_up,
    expert_down,
    dense_gate,
    dense_up,
    dense_down,
    dense_mix,
):
    tp_count = lax.axis_size("tp")
    ep_count = lax.axis_size("ep")
    tp_place = lax.axis_index("tp")
    seq_local, width = hidden.shape
    heads_local = state_matrix.shape[1]
    head_width = state_matrix.shape[2]
    part_width = width // tp_count
    feature_first = tp_place * part_width
    start_f = hidden.astype(jnp.float32)
    normed_in = (
        start_f
        * lax.rsqrt(jnp.mean(start_f * start_f, axis=-1, keepdims=True) + EPS)
        * norm_gains[0]
    ).astype(jnp.bfloat16)
    query_f = jnp.dot(normed_in, w_query, preferred_element_type=jnp.float32)
    key_f = jnp.dot(normed_in, w_key, preferred_element_type=jnp.float32)
    value_f = jnp.dot(normed_in, w_value, preferred_element_type=jnp.float32)
    gate_f = jnp.dot(normed_in, w_outgate, preferred_element_type=jnp.float32)
    head_first = tp_place * heads_local
    input_weight = lax.dynamic_slice_in_dim(w_input_gate, head_first, heads_local, 1)
    forget_weight = lax.dynamic_slice_in_dim(w_forget_gate, head_first, heads_local, 1)
    forget_local = lax.dynamic_slice_in_dim(forget_bias, head_first, heads_local, 0)
    in_gate = jnp.dot(normed_in, input_weight, preferred_element_type=jnp.float32)
    log_forget = jax.nn.log_sigmoid(
        jnp.dot(normed_in, forget_weight, preferred_element_type=jnp.float32) + forget_local
    )
    query = settle(query_f).reshape(seq_local, heads_local, head_width)
    keys = settle(key_f).reshape(seq_local, heads_local, head_width) * head_width ** (-0.5)
    values = settle(value_f).reshape(seq_local, heads_local, head_width)
    carried = log_forget + state_max
    new_max = jnp.maximum(carried, in_gate)
    keep = jnp.exp(carried - new_max)
    write = jnp.exp(in_gate - new_max)
    written = write[:, :, None] * keys
    new_matrix = (
        keep[:, :, None, None] * state_matrix + written[:, :, :, None] * values[:, :, None, :]
    )
    new_norm = keep[:, :, None] * state_norm + written
    numer = jnp.einsum("shd,shdv->shv", query, new_matrix)
    denom = jnp.einsum("shd,shd->sh", query, new_norm)
    read = numer / jnp.maximum(jnp.abs(denom), jnp.exp(-new_max))[:, :, None]
    mixed = (
        jax.nn.sigmoid(settle(gate_f)) * read.reshape(seq_local, heads_local * head_width)
    ).astype(jnp.bfloat16)
    branch_terms = settle(jnp.dot(mixed, w_mix_out, preferred_element_type=jnp.float32))
    branch = settle(
        lax.psum_scatter(
            branch_terms.astype(jnp.bfloat16), "tp", scatter_dimension=1, tiled=True
        ).astype(jnp.float32)
    )
    start_part = lax.dynamic_slice_in_dim(start_f, feature_first, part_width, 1)
    gain_rows = lax.dynamic_slice_in_dim(norm_gains, feature_first, part_width, 1)
    lifted = gain_rows[1] * branch
    mix_weight = gain_rows[2] * lax.dynamic_slice_in_dim(dense_mix, feature_first, part_width, 0)
    branch_sq, start_sq, cross_sum, lifted_sq, start_dot, lifted_dot = lax.psum(
        (
            jnp.sum(branch * branch, axis=-1),
            jnp.sum(start_part * start_part, axis=-1),
            jnp.sum(start_part * lifted, axis=-1),
            jnp.sum(lifted * lifted, axis=-1),
            jnp.sum(start_part * mix_weight, axis=-1),
            jnp.sum(lifted * mix_weight, axis=-1),
        ),
        "tp",
    )
    branch_scale = lax.rsqrt(branch_sq / width + EPS)
    residual_f = start_part + lifted * branch_scale[:, None]
    resid_sq = start_sq + 2.0 * branch_scale * cross_sum + branch_scale * branch_scale * lifted_sq
    gate_dot = start_dot + branch_scale * lifted_dot
    scale_two = lax.rsqrt(resid_sq / width + EPS)
    mix_gate = jax.nn.sigmoid(scale_two * gate_dot)
    residual = settle(residual_f)
    normed = (residual_f * scale_two[:, None] * gain_rows[2]).astype(jnp.bfloat16)
    rows_in = lax.all_gather(normed, "ep", axis=0, tiled=True)
    dense_pre = jnp.concatenate(
        [
            jnp.dot(rows_in, dense_gate, preferred_element_type=jnp.float32),
            jnp.dot(rows_in, dense_up, preferred_element_type=jnp.float32),
        ],
        axis=1,
    )
    dense_pre = lax.psum(dense_pre.astype(jnp.bfloat16), "tp").astype(jnp.float32)
    dense_pre_gate, dense_pre_up = jnp.split(dense_pre, 2, axis=1)
    dense_hidden = (jax.nn.silu(dense_pre_gate) * dense_pre_up).astype(jnp.bfloat16)
    dense_out = lax.psum_scatter(
        jnp.dot(dense_hidden, dense_down, preferred_element_type=jnp.float32).astype(jnp.bfloat16),
        "ep",
        scatter_dimension=0,
        tiled=True,
    ).astype(jnp.float32)
    route_width = routes.shape[1]
    expert_count = ep_count * expert_gate.shape[0]
    capacity = 2 * seq_local * route_width // ep_count
    flat_expert = routes.reshape(-1)
    picks = (flat_expert[:, None] == jnp.arange(expert_count, dtype=jnp.int32)[None, :]).astype(
        jnp.int32
    )
    ranks = jnp.sum(jnp.cumsum(picks, axis=0) * picks, axis=1) - 1
    slot_index = flat_expert * capacity + ranks
    placing = (
        jnp.arange(expert_count * capacity, dtype=jnp.int32)[:, None] == slot_index[None, :]
    ).astype(jnp.bfloat16)
    repeated = jnp.repeat(normed, route_width, axis=0)
    outgoing = (
        jnp.dot(placing, repeated, preferred_element_type=jnp.float32)
        .astype(jnp.bfloat16)
        .reshape(expert_count, capacity, part_width)
    )
    arrived = lax.all_to_all(outgoing, "ep", split_axis=0, concat_axis=0, tiled=True)
    full_rows = lax.all_gather(arrived, "tp", axis=2, tiled=True)
    flat_rows = full_rows.reshape(-1, width)
    gate_pre = jnp.dot(flat_rows, expert_gate[0], preferred_element_type=jnp.float32)
    up_pre = jnp.dot(flat_rows, expert_up[0], preferred_element_type=jnp.float32)
    hidden_units = (jax.nn.silu(gate_pre) * up_pre).astype(jnp.bfloat16)
    partial_out = settle(jnp.dot(hidden_units, expert_down[0], preferred_element_type=jnp.float32))
    summed_out = lax.psum_scatter(
        partial_out.astype(jnp.bfloat16), "tp", scatter_dimension=1, tiled=True
    )
    returned = lax.all_to_all(
        summed_out.reshape(arrived.shape), "ep", split_axis=0, concat_axis=0, tiled=True
    )
    picked = lax.dot_general(
        placing,
        returned.reshape(expert_count * capacity, part_width),
        (((0,), (0,)), ((), ())),
        preferred_element_type=jnp.float32,
    )
    share = route_scores / jnp.sum(route_scores, axis=-1, keepdims=True)
    moe_out = jnp.sum(
        picked.reshape(seq_local, route_width, part_width) * share[:, :, None], axis=1
    )
    ffn = moe_out + mix_gate[:, None] * dense_out
    ffn_sq = lax.psum(jnp.sum(ffn * ffn, axis=-1), "tp")
    new_hidden = (residual + gain_rows[3] * ffn * lax.rsqrt(ffn_sq / width + EPS)[:, None]).astype(
        jnp.bfloat16
    )
    return (new_hidden, new_matrix, new_norm, new_max)


def solution(mesh):
    placed = (
        P("ep", None),
        P(),
        P(None, "tp"),
        P(None, "tp"),
        P(None, "tp"),
        P(None, "tp"),
        P(),
        P(),
        P(),
        P("tp", None),
        P("ep", "tp", None, None),
        P("ep", "tp", None),
        P("ep", "tp"),
        P("ep", None),
        P("ep", None),
        P("ep", None, "tp"),
        P("ep", None, "tp"),
        P("ep", "tp", None),
        P("tp", "ep"),
        P("tp", "ep"),
        P("ep", "tp"),
        P(),
    )
    return jax.shard_map(
        local,
        mesh=mesh,
        in_specs=placed,
        out_specs=(P("ep", "tp"), P("ep", "tp", None, None), P("ep", "tp", None), P("ep", "tp")),
        check_vma=False,
    )
```

profile of v0, /device:TPU:0, one launch (start us, length us, event | category | flops | bytes accessed | tf_op | source)
XLA Modules:
  0.0 237.0 jit_solution(14512095781934341025)
XLA Ops:
  9.2 1.6 convolution_convert_fusion.7
  10.9 1.1 fusion.44
  12.8 1.2 subtract_exponential_fusion
  14.1 1.6 convolution_convert_fusion.6
  15.8 1.6 convolution_convert_fusion.5
  18.7 3.7 %multiply_add_fusion = f32[32,2,128,128]{3,2,1,0:T(8,128)S(1)} fusion(f32[32,2,128,128]{3,2,1,0:T(8,128)} %param.32, f32[32,2,128]{2,1,0:T(2,128)S(1)} %reshape.112, f32[32,2,128]{2,1,0:T(2,128)S(1)} %get-tuple-element.20, f32[32,2]{1,0:T(8,128)S(1)} %copy.31), kind=kLoop, calls=%fused_computation | loop fusion | flops 3145728 | bytes 8454400 | tf_op jit(solution)/shard_map/add | solution.py:72
  22.5 2.0 copy-done.1
  28.5 20.2 %reduce-scatter.4.cloned.1.call-done = bf16[32,512]{1,0:T(8,128)(2,1)} async-done(((bf16[32,2048]{1,0:T(8,128)(2,1)}), bf16[32,512]{1,0:T(8,128)(2,1)}) %reduce-scatter.4.cloned.1.call-update) | async-done | bytes 32784 | tf_op jit(solution)/shard_map/reduce_scatter | solution.py:83
  49.7 5.8 %all-reduce = (f32[32]{0:T(128)S(1)}, f32[32]{0:T(128)S(1)}, f32[32]{0:T(128)S(1)}, f32[32]{0:T(128)S(1)}, f32[32]{0:T(128)S(1)}, /*index=5*/f32[32]{0:T(128)S(1)}) all-reduce(f32[32]{0:T(128)S(1)} %get-tuple-element.9, f32[32]{0:T(128)S(1)} %get-tuple-element.8, f32[32]{0:T(128)S(1)} %get-tuple-element.5, ...), channel_id=1, replica_groups=mesh['ep'=8,'tp'=4] {'tp'}, use_global_device_ids=true, to_apply=%region_3.4 | all-reduce | flops 192 | bytes 1536 | tf_op jit(solution)/shard_map/psum | solution.py:91
  56.3 31.2 %all_gather.7 = bf16[256,512]{1,0:T(8,128)(2,1)S(1)} all-gather(bf16[32,512]{1,0:T(8,128)(2,1)S(1)} %get-tuple-element.23), channel_id=1, replica_groups=mesh['ep'=8,'tp'=4] {'ep'}, dimensions={0}, use_global_device_ids=true | all-gather | bytes 294912 | tf_op jit(solution)/shard_map/all_gather | solution.py:110
  89.2 5.3 %all-to-all-start = ((bf16[8,16,512]{2,1,0:T(8,128)(2,1)}), bf16[8,16,512]{2,1,0:T(8,128)(2,1)S(1)}, u32[]{:S(2)}, u32[]{:S(2)}) async-start(bf16[8,16,512]{2,1,0:T(8,128)(2,1)} %bitcast.6), calls=%async_computation.1 | async-start | bytes 262144 | tf_op jit(solution)/shard_map/all_to_all | solution.py:145
  95.5 6.3 %all-to-all-done = bf16[8,16,512]{2,1,0:T(8,128)(2,1)S(1)} async-done(((bf16[8,16,512]{2,1,0:T(8,128)(2,1)}), bf16[8,16,512]{2,1,0:T(8,128)(2,1)S(1)}, u32[]{:S(2)}, u32[]{:S(2)}) %all-to-all-start) | async-done | bytes 131104 | tf_op jit(solution)/shard_map/all_to_all | solution.py:145
  101.8 9.2 %all_gather.6 = bf16[8,16,2048]{2,1,0:T(8,128)(2,1)S(1)} all-gather(bf16[8,16,512]{2,1,0:T(8,128)(2,1)S(1)} %all-to-all-done), channel_id=1, replica_groups=mesh['ep'=8,'tp'=4] {'tp'}, dimensions={2}, use_global_device_ids=true | all-gather | bytes 655360 | tf_op jit(solution)/shard_map/all_gather | solution.py:146
  111.0 2.8 %fusion.4 = f32[128,896]{1,0:T(8,128)S(1)} fusion(bf16[128,2048]{1,0:T(8,128)(2,1)S(1)} %bitcast.51, bf16[1,2048,896]{2,1,0:T(8,128)(2,1)} %param.37), kind=kOutput, calls=%fused_computation.5 | convolution fusion | flops 469762048 | bytes 4653056 | tf_op jit(solution)/shard_map/dot_general | solution.py:148
  113.9 5.5 %fusion.6 = bf16[128,2048]{1,0:T(8,128)(2,1)} fusion(bf16[1,896,2048]{2,1,0:T(8,128)(2,1)} %param.39, bf16[128,2048]{1,0:T(8,128)(2,1)S(1)} %bitcast.52, bf16[1,2048,896]{2,1,0:T(8,128)(2,1)} %param.38, f32[128,896]{1,0:T(8,128)S(1)} %fusion.4), kind=kOutput, calls=%fused_computation.7 | convolution fusion | flops 940474368 | bytes 8847360 | tf_op jit(solution)/shard_map/dot_general | solution.py:151
  119.4 13.2 %all-reduce.3.cloned.1.call-done = bf16[256,1408]{0,1:T(8,128)(2,1)} async-done(((bf16[256,1408]{0,1:T(8,128)(2,1)}), bf16[256,1408]{0,1:T(8,128)(2,1)}) %all-reduce.3.cloned.1.call-update) | async-done | bytes 720912 | tf_op jit(solution)/shard_map/psum | solution.py:118
  132.6 1.2 convert_element_type.94
  133.8 1.1 convolution_convert_fusion.3
  134.9 21.8 %reduce-scatter.6.cloned.1.call-done = bf16[128,512]{1,0:T(8,128)(2,1)} async-done(((bf16[128,2048]{1,0:T(8,128)(2,1)}), bf16[128,512]{1,0:T(8,128)(2,1)}) %reduce-scatter.6.cloned.1.call-update) | async-done | bytes 131088 | tf_op jit(solution)/shard_map/reduce_scatter | solution.py:152
  156.7 5.5 %all-to-all-start.1 = ((bf16[8,16,512]{2,1,0:T(8,128)(2,1)}), bf16[8,16,512]{2,1,0:T(8,128)(2,1)S(1)}, u32[]{:S(2)}, u32[]{:S(2)}) async-start(bf16[8,16,512]{2,1,0:T(8,128)(2,1)} %bitcast.62), calls=%async_computation.3 | async-start | bytes 262144 | tf_op jit(solution)/shard_map/all_to_all | solution.py:155
  162.4 7.2 %all-to-all-done.1 = bf16[8,16,512]{2,1,0:T(8,128)(2,1)S(1)} async-done(((bf16[8,16,512]{2,1,0:T(8,128)(2,1)}), bf16[8,16,512]{2,1,0:T(8,128)(2,1)S(1)}, u32[]{:S(2)}, u32[]{:S(2)}) %all-to-all-start.1) | async-done | bytes 131104 | tf_op jit(solution)/shard_map/all_to_all | solution.py:155
  169.8 52.6 %reduce-scatter.8.cloned.1.call-done = bf16[32,512]{1,0:T(8,128)(2,1)} async-done(((bf16[256,512]{1,0:T(8,128)(2,1)}), bf16[32,512]{1,0:T(8,128)(2,1)}) %reduce-scatter.8.cloned.1.call-update) | async-done | bytes 32784 | tf_op jit(solution)/shard_map/reduce_scatter | solution.py:121
  223.3 5.7 %psum.63 = f32[32]{0:T(128)S(1)} all-reduce(f32[32]{0:T(128)S(1)} %multiply_reduce_fusion.1), channel_id=1, replica_groups=mesh['ep'=8,'tp'=4] {'tp'}, use_global_device_ids=true, to_apply=%region_22.23 | all-reduce | flops 32 | bytes 256 | tf_op jit(solution)/shard_map/psum | solution.py:169
  229.0 1.5 add_convert_fusion
  (73 shorter events, 14.0 us)
Async XLA Ops:
  7.2 18.1 %copy-start = (bf16[256,2048]{1,0:T(8,128)(2,1)S(1)}, bf16[256,2048]{1,0:T(8,128)(2,1)}, u32[]{:S(2)}) copy-start(bf16[256,2048]{1,0:T(8,128)(2,1)} %param.31) | copy-start | bytes 3145732
  7.2 11.2 %copy-start.2 = (bf16[32,2048]{1,0:T(8,128)(2,1)S(1)}, bf16[32,2048]{1,0:T(8,128)(2,1)}, u32[]{:S(2)}) copy-start(bf16[32,2048]{1,0:T(8,128)(2,1)} %param.22) | copy-start | bytes 393220
  7.2 10.3 %copy-start.6 = (f32[32,2,128]{2,1,0:T(2,128)S(1)}, f32[32,2,128]{2,1,0:T(2,128)}, u32[]{:S(2)}) copy-start(f32[32,2,128]{2,1,0:T(2,128)} %param.33) | copy-start | bytes 98308
  7.2 11.2 %copy-start.3 = (bf16[2048,256]{1,0:T(8,128)(2,1)S(1)}, bf16[2048,256]{1,0:T(8,128)(2,1)}, u32[]{:S(2)}) copy-start(bf16[2048,256]{1,0:T(8,128)(2,1)} %param.27) | copy-start | bytes 3145732
  7.2 41.5 %reduce-scatter.4.cloned.1.call-start = ((), (), s32[]{:S(2)}) async-start(), calls=%async_computation.5 | async-start | bytes 163840 | tf_op jit(solution)/shard_map/reduce_scatter | solution.py:83
  13.9 8.5 %copy-start.7 = (f32[32,2]{0,1:T(2,128)}, f32[32,2]{0,1:T(2,128)S(1)}, u32[]{:S(2)}) copy-start(f32[32,2]{0,1:T(2,128)S(1)} %get-tuple-element.22) | copy-start | bytes 772
  22.4 2.0 copy-start.1
  24.5 1.7 copy-start.9
  24.5 63.0 %copy-start.4 = (bf16[512,704]{0,1:T(8,128)(2,1)S(1)}, bf16[512,704]{0,1:T(8,128)(2,1)}, u32[]{:S(2)}) copy-start(bf16[512,704]{0,1:T(8,128)(2,1)} %param.41) | copy-start | bytes 2162692
  24.5 63.4 %copy-start.5 = (bf16[512,704]{0,1:T(8,128)(2,1)S(1)}, bf16[512,704]{0,1:T(8,128)(2,1)}, u32[]{:S(2)}) copy-start(bf16[512,704]{0,1:T(8,128)(2,1)} %param.40) | copy-start | bytes 2162692
  89.2 12.6 %all-to-all-start = ((bf16[8,16,512]{2,1,0:T(8,128)(2,1)}), bf16[8,16,512]{2,1,0:T(8,128)(2,1)S(1)}, u32[]{:S(2)}, u32[]{:S(2)}) async-start(bf16[8,16,512]{2,1,0:T(8,128)(2,1)} %bitcast.6), calls=%async_computation.1 | async-start | bytes 262144 | tf_op jit(solution)/shard_map/all_to_all | solution.py:145
  94.5 38.1 %all-reduce.3.cloned.1.call-start = ((), (), s32[]{:S(2)}) async-start(), calls=%async_computation.7 | async-start | bytes 1441792 | tf_op jit(solution)/shard_map/psum | solution.py:118
  95.5 61.3 %reduce-scatter.6.cloned.1.call-start = ((), (), s32[]{:S(2)}) async-start(), calls=%async_computation.6 | async-start | bytes 655360 | tf_op jit(solution)/shard_map/reduce_scatter | solution.py:152
  113.8 19.9 %copy-start.10 = (bf16[704,512]{1,0:T(8,128)(2,1)S(1)}, bf16[704,512]{1,0:T(8,128)(2,1)}, u32[]{:S(2)}) copy-start(bf16[704,512]{1,0:T(8,128)(2,1)} %param.42) | copy-start | bytes 2162692
  119.3 43.0 %copy-start.8 = (f32[32,2]{0,1:T(2,128)S(1)}, f32[32,2]{0,1:T(2,128)}, u32[]{:S(2)}) copy-start(f32[32,2]{0,1:T(2,128)} %param.36) | copy-start | bytes 772
  119.3 103.0 %reduce-scatter.8.cloned.1.call-start = ((), (), s32[]{:S(2)}) async-start(), calls=%async_computation.8 | async-start | bytes 294912 | tf_op jit(solution)/shard_map/reduce_scatter | solution.py:121
  156.7 12.9 %all-to-all-start.1 = ((bf16[8,16,512]{2,1,0:T(8,128)(2,1)}), bf16[8,16,512]{2,1,0:T(8,128)(2,1)S(1)}, u32[]{:S(2)}, u32[]{:S(2)}) async-start(bf16[8,16,512]{2,1,0:T(8,128)(2,1)} %bitcast.62), calls=%async_computation.3 | async-start | bytes 262144 | tf_op jit(solution)/shard_map/all_to_all | solution.py:155
Sparse Core Ops, SparseCore 0:
  26.3 22.3 reduce-scatter.3
  97.7 34.8 all-reduce.2
  135.0 21.6 reduce-scatter.5
  159.9 62.4 reduce-scatter.7
where the time goes:
time: 238 us; the launch traced here: 237 us
  waiting for transfers between devices  121 us (51%)
  blocking collectives  51.8 us (22%)
  matrix products  20.2 us (8%)
  between operations  14.1 us (6%)
  other arithmetic  13.3 us (6%)
  starting transfers between devices  11 us (5%)
  local copies, waits for them, and re-layouts  5.31 us (2%)
    reduce_scatter x1, waiting for transfers between devices, local(): lax.psum_scatter(jnp.dot(dense_hidden, dense_down, preferred_element_type...  52.6 us
    all_gather x1, blocking collectives, local(): rows_in = lax.all_gather(normed, 'ep', axis=0, tiled=True)  31.2 us
    reduce_scatter x1, waiting for transfers between devices, local(): lax.psum_scatter(partial_out.astype(jnp.bfloat16), 'tp', scatter_dimensio...  21.8 us
    reduce_scatter x1, waiting for transfers between devices, local(): lax.psum_scatter(branch_terms.astype(jnp.bfloat16), 'tp', scatter_dimensi...  20.2 us
    psum x1, waiting for transfers between devices, local(): lax.psum(dense_pre.astype(jnp.bfloat16), 'tp').astype(jnp.float32)  13.2 us
    all_gather x1, blocking collectives, local(): full_rows = lax.all_gather(arrived, 'tp', axis=2, tiled=True)  9.21 us
    all_to_all x1, waiting for transfers between devices, local(): lax.all_to_all(summed_out.reshape(arrived.shape), 'ep', split_axis=0, con...  7.21 us
    all_to_all x1, waiting for transfers between devices, local(): lax.all_to_all(outgoing, 'ep', split_axis=0, concat_axis=0, tiled=True)  6.31 us
  transfers between devices with their start and end apart: 6, of which 6 were waited for; matrix products, arithmetic and copies ran while one was open for 6% of the time, Pallas kernels for 0%

commit v1 on v0

--- a/solution.py
+++ b/solution.py
@@ -4,6 +4,18 @@
 from jax.sharding import PartitionSpec as P
 
 EPS = 1e-06
+
+
+def collect(value, axis, dim):
+    ways, here, step = (lax.axis_size(axis), lax.axis_index(axis), value.shape[dim])
+    line, have = (value, 1)
+    while have < ways:
+        line = jnp.concatenate(
+            [line, lax.ppermute(line, axis, [(d, (d - have) % ways) for d in range(ways)])],
+            axis=dim,
+        )
+        have = 2 * have
+    return jnp.roll(line, here * step, axis=dim)
 
 
 def settle(values):
@@ -107,7 +119,7 @@
     mix_gate = jax.nn.sigmoid(scale_two * gate_dot)
     residual = settle(residual_f)
     normed = (residual_f * scale_two[:, None] * gain_rows[2]).astype(jnp.bfloat16)
-    rows_in = lax.all_gather(normed, "ep", axis=0, tiled=True)
+    rows_in = collect(normed, "ep", 0)
     dense_pre = jnp.concatenate(
         [
             jnp.dot(rows_in, dense_gate, preferred_element_type=jnp.float32),

time: 238 us -> 221 us (0.929)
  blocking collectives: 51.8 us -> 17.9 us
  starting transfers between devices: 11 us -> 19.9 us
  waiting for transfers between devices: 121 us -> 128 us
    all_gather x1 -> x0, blocking collectives: 31.2 us -> none  [local(): rows_in = lax.all_gather(normed, 'ep', axis=0, tiled=True)]
    ppermute x0 -> x3, starting transfers between devices: none -> 8.84 us  [collect(): lax.ppermute(line, axis, [(d, (d - have) % ways) for d in range(ways)])]
    ppermute x0 -> x3, waiting for transfers between devices: none -> 8.51 us  [collect(): lax.ppermute(line, axis, [(d, (d - have) % ways) for d in range(ways)])]
    all_to_all x1, waiting for transfers between devices: 6.31 us -> 0.01 us  [local(): lax.all_to_all(outgoing, 'ep', split_axis=0, concat_axis=0, tiled=True)]
    psum x1, waiting for transfers between devices: 13.2 us -> 18.3 us  [local(): lax.psum(dense_pre.astype(jnp.bfloat16), 'tp').astype(jnp.float32)]
    all_gather x1, blocking collectives: 9.21 us -> 6.5 us  [local(): full_rows = lax.all_gather(arrived, 'tp', axis=2, tiled=True)]
  transfers between devices with their start and end apart: 6 -> 9, of which waited for: 6 -> 7; matrix products, arithmetic and copies ran while one was open for 6% -> 8% of each run, Pallas kernels for 0% -> 0%
where the time goes in v1:
time: 221 us; the launch traced here: 220 us
  waiting for transfers between devices  128 us (58%)
  matrix products  21.2 us (10%)
  starting transfers between devices  19.9 us (9%)
  blocking collectives  17.9 us (8%)
  between operations  14.1 us (6%)
  other arithmetic  14 us (6%)
  local copies, waits for them, and re-layouts  5.36 us (2%)
    reduce_scatter x1, waiting for transfers between devices, local(): lax.psum_scatter(jnp.dot(dense_hidden, dense_down, preferred_element_type...  52.6 us
    reduce_scatter x1, waiting for transfers between devices, local(): lax.psum_scatter(partial_out.astype(jnp.bfloat16), 'tp', scatter_dimensio...  20.7 us
    reduce_scatter x1, waiting for transfers between devices, local(): lax.psum_scatter(branch_terms.astype(jnp.bfloat16), 'tp', scatter_dimensi...  20.3 us
    psum x1, waiting for transfers between devices, local(): lax.psum(dense_pre.astype(jnp.bfloat16), 'tp').astype(jnp.float32)  18.3 us
    ppermute x3, starting transfers between devices, collect(): lax.ppermute(line, axis, [(d, (d - have) % ways) for d in range(ways)])  8.84 us
    ppermute x3, waiting for transfers between devices, collect(): lax.ppermute(line, axis, [(d, (d - have) % ways) for d in range(ways)])  8.51 us
    all_to_all x1, waiting for transfers between devices, local(): lax.all_to_all(summed_out.reshape(arrived.shape), 'ep', split_axis=0, con...  7.23 us
    all_gather x1, blocking collectives, local(): full_rows = lax.all_gather(arrived, 'tp', axis=2, tiled=True)  6.5 us
  transfers between devices with their start and end apart: 9, of which 7 were waited for; matrix products, arithmetic and copies ran while one was open for 8% of the time, Pallas kernels for 0%

profile of v1, /device:TPU:0, one launch (start us, length us, event | category | flops | bytes accessed | tf_op | source)
XLA Modules:
  0.0 220.2 jit_solution(6210317358927325782)
XLA Ops:
  9.2 1.6 convolution_convert_fusion.7
  10.9 1.6 convolution_convert_fusion.5
  15.7 1.6 convolution_convert_fusion.6
  18.7 3.7 %multiply_add_fusion = f32[32,2,128,128]{3,2,1,0:T(8,128)S(1)} fusion(f32[32,2,128,128]{3,2,1,0:T(8,128)} %param.32, f32[32,2,128]{2,1,0:T(2,128)S(1)} %reshape.112, f32[32,2,128]{2,1,0:T(2,128)S(1)} %get-tuple-element.22, f32[32,2]{1,0:T(8,128)S(1)} %copy.31), kind=kLoop, calls=%fused_computation | loop fusion | flops 3145728 | bytes 8454400 | tf_op jit(solution)/shard_map/add | solution.py:84
  22.5 2.0 copy-done.1
  28.4 20.3 %reduce-scatter.4.cloned.1.call-done = bf16[32,512]{1,0:T(8,128)(2,1)} async-done(((bf16[32,2048]{1,0:T(8,128)(2,1)}), bf16[32,512]{1,0:T(8,128)(2,1)}) %reduce-scatter.4.cloned.1.call-update) | async-done | bytes 32784 | tf_op jit(solution)/shard_map/reduce_scatter | solution.py:95
  49.7 5.8 %all-reduce = (f32[32]{0:T(128)S(1)}, f32[32]{0:T(128)S(1)}, f32[32]{0:T(128)S(1)}, f32[32]{0:T(128)S(1)}, f32[32]{0:T(128)S(1)}, /*index=5*/f32[32]{0:T(128)S(1)}) all-reduce(f32[32]{0:T(128)S(1)} %get-tuple-element.9, f32[32]{0:T(128)S(1)} %get-tuple-element.8, f32[32]{0:T(128)S(1)} %get-tuple-element.5, ...), channel_id=1, replica_groups=mesh['ep'=8,'tp'=4] {'tp'}, use_global_device_ids=true, to_apply=%region_3.4 | all-reduce | flops 192 | bytes 1536 | tf_op jit(solution)/shard_map/psum | solution.py:103
  56.3 4.4 %collective-permute-start = (bf16[32,512]{1,0:T(8,128)(2,1)S(1)}, bf16[32,512]{1,0:T(8,128)(2,1)S(1)}, u32[]{:S(2)}, u32[]{:S(2)}) collective-permute-start(bf16[32,512]{1,0:T(8,128)(2,1)S(1)} %get-tuple-element.19), channel_id=1, source_target_pairs={{0,28},{4,0},{8,4},{12,8},{16,12},{20,16},{24,20},{28,24},{1,29},{... | collective-permute-start | bytes 98312 | tf_op jit(solution)/shard_map/ppermute | solution.py:14
  60.8 1.5 collective-permute-done
  63.0 1.4 collective-permute-start.1
  65.3 5.4 %all-to-all-start = ((bf16[8,16,512]{2,1,0:T(8,128)(2,1)}), bf16[8,16,512]{2,1,0:T(8,128)(2,1)S(1)}, u32[]{:S(2)}, u32[]{:S(2)}) async-start(bf16[8,16,512]{2,1,0:T(8,128)(2,1)} %bitcast.51), calls=%async_computation.1 | async-start | bytes 262144 | tf_op jit(solution)/shard_map/all_to_all | solution.py:157
  70.7 2.9 %collective-permute-start.2 = (bf16[128,512]{1,0:T(8,128)(2,1)S(1)}, bf16[128,512]{1,0:T(8,128)(2,1)S(1)}, u32[]{:S(2)}, u32[]{:S(2)}) collective-permute-start(bf16[128,512]{1,0:T(8,128)(2,1)S(1)} %pad_maximum_fusion.1), channel_id=1, source_target_pairs={{0,16},{4,20},{8,24},{12,28},{16,0},{20,4},{24,8},{28,12},{1,17},{... | collective-permute-start | bytes 393224 | tf_op jit(solution)/shard_map/ppermute | solution.py:14
  73.7 7.0 %collective-permute-done.2 = bf16[128,512]{1,0:T(8,128)(2,1)S(1)} collective-permute-done((bf16[128,512]{1,0:T(8,128)(2,1)S(1)}, bf16[128,512]{1,0:T(8,128)(2,1)S(1)}, u32[]{:S(2)}, u32[]{:S(2)}) %collective-permute-start.2) | collective-permute-done | bytes 131104 | tf_op jit(solution)/shard_map/ppermute | solution.py:14
  82.6 6.5 %all_gather.3 = bf16[8,16,2048]{2,1,0:T(8,128)(2,1)S(1)} all-gather(bf16[8,16,512]{2,1,0:T(8,128)(2,1)S(1)} %all-to-all-done), channel_id=1, replica_groups=mesh['ep'=8,'tp'=4] {'tp'}, dimensions={2}, use_global_device_ids=true | all-gather | bytes 655360 | tf_op jit(solution)/shard_map/all_gather | solution.py:158
  89.1 2.8 %fusion.4 = f32[128,896]{1,0:T(8,128)S(1)} fusion(bf16[128,2048]{1,0:T(8,128)(2,1)S(1)} %bitcast.49, bf16[1,2048,896]{2,1,0:T(8,128)(2,1)} %param.37), kind=kOutput, calls=%fused_computation.5 | convolution fusion | flops 469762048 | bytes 4653056 | tf_op jit(solution)/shard_map/dot_general | solution.py:160
  91.9 5.4 %fusion.6 = bf16[128,2048]{1,0:T(8,128)(2,1)} fusion(bf16[1,896,2048]{2,1,0:T(8,128)(2,1)} %param.39, bf16[128,2048]{1,0:T(8,128)(2,1)S(1)} %bitcast.50, bf16[1,2048,896]{2,1,0:T(8,128)(2,1)} %param.38, f32[128,896]{1,0:T(8,128)S(1)} %fusion.4), kind=kOutput, calls=%fused_computation.7 | convolution fusion | flops 940474368 | bytes 8847360 | tf_op jit(solution)/shard_map/dot_general | solution.py:163
  97.4 18.3 %all-reduce.3.cloned.1.call-done = bf16[256,1408]{0,1:T(8,128)(2,1)} async-done(((bf16[256,1408]{0,1:T(8,128)(2,1)}), bf16[256,1408]{0,1:T(8,128)(2,1)}) %all-reduce.3.cloned.1.call-update) | async-done | bytes 720912 | tf_op jit(solution)/shard_map/psum | solution.py:130
  116.9 2.2 %convolution_convert_fusion.3 = bf16[256,512]{1,0:T(8,128)(2,1)} fusion(bf16[704,512]{1,0:T(8,128)(2,1)} %param.42, f32[256,1408]{0,1:T(8,128)S(1)} %convert_element_type.94), kind=kOutput, calls=%fused_computation.12 | convolution fusion | flops 185761792 | bytes 2424832 | tf_op jit(solution)/shard_map/dot_general | solution.py:134
  119.2 20.7 %reduce-scatter.6.cloned.1.call-done = bf16[128,512]{1,0:T(8,128)(2,1)} async-done(((bf16[128,2048]{1,0:T(8,128)(2,1)}), bf16[128,512]{1,0:T(8,128)(2,1)}) %reduce-scatter.6.cloned.1.call-update) | async-done | bytes 131088 | tf_op jit(solution)/shard_map/reduce_scatter | solution.py:164
  139.9 5.5 %all-to-all-start.1 = ((bf16[8,16,512]{2,1,0:T(8,128)(2,1)}), bf16[8,16,512]{2,1,0:T(8,128)(2,1)S(1)}, u32[]{:S(2)}, u32[]{:S(2)}) async-start(bf16[8,16,512]{2,1,0:T(8,128)(2,1)} %bitcast.61), calls=%async_computation.3 | async-start | bytes 262144 | tf_op jit(solution)/shard_map/all_to_all | solution.py:167
  145.6 7.2 %all-to-all-done.1 = bf16[8,16,512]{2,1,0:T(8,128)(2,1)S(1)} async-done(((bf16[8,16,512]{2,1,0:T(8,128)(2,1)}), bf16[8,16,512]{2,1,0:T(8,128)(2,1)S(1)}, u32[]{:S(2)}, u32[]{:S(2)}) %all-to-all-start.1) | async-done | bytes 131104 | tf_op jit(solution)/shard_map/all_to_all | solution.py:167
  153.0 52.6 %reduce-scatter.8.cloned.1.call-done = bf16[32,512]{1,0:T(8,128)(2,1)} async-done(((bf16[256,512]{1,0:T(8,128)(2,1)}), bf16[32,512]{1,0:T(8,128)(2,1)}) %reduce-scatter.8.cloned.1.call-update) | async-done | bytes 32784 | tf_op jit(solution)/shard_map/reduce_scatter | solution.py:133
  206.5 5.7 %psum.63 = f32[32]{0:T(128)S(1)} all-reduce(f32[32]{0:T(128)S(1)} %multiply_reduce_fusion.1), channel_id=1, replica_groups=mesh['ep'=8,'tp'=4] {'tp'}, use_global_device_ids=true, to_apply=%region_22.23 | all-reduce | flops 32 | bytes 256 | tf_op jit(solution)/shard_map/psum | solution.py:181
  212.2 1.5 add_convert_fusion
  (92 shorter events, 18.3 us)
Async XLA Ops:
  7.2 18.1 %copy-start = (bf16[256,2048]{1,0:T(8,128)(2,1)S(1)}, bf16[256,2048]{1,0:T(8,128)(2,1)}, u32[]{:S(2)}) copy-start(bf16[256,2048]{1,0:T(8,128)(2,1)} %param.31) | copy-start | bytes 3145732
  7.2 11.2 %copy-start.2 = (bf16[32,2048]{1,0:T(8,128)(2,1)S(1)}, bf16[32,2048]{1,0:T(8,128)(2,1)}, u32[]{:S(2)}) copy-start(bf16[32,2048]{1,0:T(8,128)(2,1)} %param.22) | copy-start | bytes 393220
  7.2 10.3 %copy-start.7 = (f32[32,2,128]{2,1,0:T(2,128)S(1)}, f32[32,2,128]{2,1,0:T(2,128)}, u32[]{:S(2)}) copy-start(f32[32,2,128]{2,1,0:T(2,128)} %param.33) | copy-start | bytes 98308
  7.2 11.2 %copy-start.3 = (bf16[2048,256]{1,0:T(8,128)(2,1)S(1)}, bf16[2048,256]{1,0:T(8,128)(2,1)}, u32[]{:S(2)}) copy-start(bf16[2048,256]{1,0:T(8,128)(2,1)} %param.27) | copy-start | bytes 3145732
  7.2 41.5 %reduce-scatter.4.cloned.1.call-start = ((), (), s32[]{:S(2)}) async-start(), calls=%async_computation.5 | async-start | bytes 163840 | tf_op jit(solution)/shard_map/reduce_scatter | solution.py:95
  15.6 6.8 %copy-start.8 = (f32[32,2]{0,1:T(2,128)}, f32[32,2]{0,1:T(2,128)S(1)}, u32[]{:S(2)}) copy-start(f32[32,2]{0,1:T(2,128)S(1)} %get-tuple-element.24) | copy-start | bytes 772
  22.4 2.0 copy-start.1
  24.5 1.7 copy-start.12
  24.5 56.3 %copy-start.4 = (bf16[512,704]{0,1:T(8,128)(2,1)S(1)}, bf16[512,704]{0,1:T(8,128)(2,1)}, u32[]{:S(2)}) copy-start(bf16[512,704]{0,1:T(8,128)(2,1)} %param.41) | copy-start | bytes 2162692
  25.1 56.1 %copy-start.5 = (bf16[512,704]{0,1:T(8,128)(2,1)S(1)}, bf16[512,704]{0,1:T(8,128)(2,1)}, u32[]{:S(2)}) copy-start(bf16[512,704]{0,1:T(8,128)(2,1)} %param.40) | copy-start | bytes 2162692
  56.3 6.0 %collective-permute-start = (bf16[32,512]{1,0:T(8,128)(2,1)S(1)}, bf16[32,512]{1,0:T(8,128)(2,1)S(1)}, u32[]{:S(2)}, u32[]{:S(2)}) collective-permute-start(bf16[32,512]{1,0:T(8,128)(2,1)S(1)} %get-tuple-element.19), channel_id=1, source_target_pairs={{0,28},{4,0},{8,4},{12,8},{16,12},{20,16},{24,20},{28,24},{1,29},{... | collective-permute-start | bytes 98312 | tf_op jit(solution)/shard_map/ppermute | solution.py:14
  60.8 4.5 %copy-start.10 = (s32[64]{0:T(128)}, s32[64]{0:T(128)S(1)}, u32[]{:S(2)}) copy-start(s32[64]{0:T(128)S(1)} %add_add_fusion) | copy-start | bytes 772
  63.0 7.7 %collective-permute-start.1 = (bf16[64,512]{1,0:T(8,128)(2,1)}, bf16[64,512]{1,0:T(8,128)(2,1)S(1)}, u32[]{:S(2)}, u32[]{:S(2)}) collective-permute-start(bf16[64,512]{1,0:T(8,128)(2,1)} %pad_maximum_fusion.2), channel_id=1, source_target_pairs={{0,24},{4,28},{8,0},{12,4},{16,8},{20,12},{24,16},{28,20},{1,25},{... | collective-permute-start | bytes 196616 | tf_op jit(solution)/shard_map/ppermute | solution.py:14
  65.3 17.3 %all-to-all-start = ((bf16[8,16,512]{2,1,0:T(8,128)(2,1)}), bf16[8,16,512]{2,1,0:T(8,128)(2,1)S(1)}, u32[]{:S(2)}, u32[]{:S(2)}) async-start(bf16[8,16,512]{2,1,0:T(8,128)(2,1)} %bitcast.51), calls=%async_computation.1 | async-start | bytes 262144 | tf_op jit(solution)/shard_map/all_to_all | solution.py:157
  70.7 45.1 %all-reduce.3.cloned.1.call-start = ((), (), s32[]{:S(2)}) async-start(), calls=%async_computation.7 | async-start | bytes 1441792 | tf_op jit(solution)/shard_map/psum | solution.py:130
  70.7 9.9 %collective-permute-start.2 = (bf16[128,512]{1,0:T(8,128)(2,1)S(1)}, bf16[128,512]{1,0:T(8,128)(2,1)S(1)}, u32[]{:S(2)}, u32[]{:S(2)}) collective-permute-start(bf16[128,512]{1,0:T(8,128)(2,1)S(1)} %pad_maximum_fusion.1), channel_id=1, source_target_pairs={{0,16},{4,20},{8,24},{12,28},{16,0},{20,4},{24,8},{28,12},{1,17},{... | collective-permute-start | bytes 393224 | tf_op jit(solution)/shard_map/ppermute | solution.py:14
  82.5 57.4 %reduce-scatter.6.cloned.1.call-start = ((), (), s32[]{:S(2)}) async-start(), calls=%async_computation.6 | async-start | bytes 655360 | tf_op jit(solution)/shard_map/reduce_scatter | solution.py:164
  91.8 5.5 %copy-start.9 = (f32[32,2]{0,1:T(2,128)S(1)}, f32[32,2]{0,1:T(2,128)}, u32[]{:S(2)}) copy-start(f32[32,2]{0,1:T(2,128)} %param.36) | copy-start | bytes 772
  91.8 5.5 %copy-start.11 = (s32[64]{0:T(128)S(1)}, s32[64]{0:T(128)}, u32[]{:S(2)}) copy-start(s32[64]{0:T(128)} %copy-done.10) | copy-start | bytes 772
  97.2 108.4 %reduce-scatter.8.cloned.1.call-start = ((), (), s32[]{:S(2)}) async-start(), calls=%async_computation.8 | async-start | bytes 294912 | tf_op jit(solution)/shard_map/reduce_scatter | solution.py:133
  97.4 48.1 %copy-start.6 = (bf16[32,512]{1,0:T(8,128)(2,1)S(1)}, bf16[32,512]{1,0:T(8,128)(2,1)}, u32[]{:S(2)}) copy-start(bf16[32,512]{1,0:T(8,128)(2,1)} %reduce-scatter.4.cloned.1.call-done) | copy-start | bytes 98308
  139.9 12.9 %all-to-all-start.1 = ((bf16[8,16,512]{2,1,0:T(8,128)(2,1)}), bf16[8,16,512]{2,1,0:T(8,128)(2,1)S(1)}, u32[]{:S(2)}, u32[]{:S(2)}) async-start(bf16[8,16,512]{2,1,0:T(8,128)(2,1)} %bitcast.61), calls=%async_computation.3 | async-start | bytes 262144 | tf_op jit(solution)/shard_map/all_to_all | solution.py:167
Sparse Core Ops, SparseCore 0:
  26.3 22.3 reduce-scatter.3
  82.6 33.0 all-reduce.2
  118.2 21.6 reduce-scatter.5
  143.1 62.4 reduce-scatter.7
